TPU v7x, 32 devices: a whole 2x2x4 slice. The times are simulated.
32 devices in a mesh: ep: 32 (over z, y, x, core).
Axes of the slice: x: 2, y: 2, z: 4, core: 2. Of those that a mesh axis runs over, the one named last changes fastest.
Arguments:
- tokens: bfloat16 [32, 2048], P('ep'), may hold values from -6 to 6
- mixer_gain: float32 [2048], replicated, may hold values from 0.1 to 1.9
- query_weight: bfloat16 [2048, 2048], P(None, 'ep'), may hold values from -0.125 to 0.125
- key_weight: bfloat16 [2048, 2048], P(None, 'ep'), may hold values from -0.125 to 0.125
- value_weight: bfloat16 [2048, 2048], P(None, 'ep'), may hold values from -0.125 to 0.125
- outgate_weight: bfloat16 [2048, 2048], P(None, 'ep'), may hold values from -0.125 to 0.125
- input_weight: bfloat16 [2048, 4], replicated, may hold values from -0.125 to 0.125
- forget_weight: bfloat16 [2048, 4], replicated, may hold values from -0.125 to 0.125
- forget_bias: float32 [4], replicated, may hold values from 0 to 4
- memory_matrix: float32 [32, 4, 512, 512], P('ep'), may hold values from -0.3 to 0.3
- memory_norm: float32 [32, 4, 512], P('ep'), may hold values from -0.3 to 0.3
- memory_max: float32 [32, 4], P('ep'), may hold values from -2 to 2
- mixer_out: bfloat16 [2048, 2048], P(None, 'ep'), may hold values from -0.125 to 0.125
- expert_gain: float32 [2048], replicated, may hold values from 0.1 to 1.9
- expert_gate: bfloat16 [32, 2048, 1024], P('ep'), may hold values from -0.125 to 0.125
- expert_up: bfloat16 [32, 2048, 1024], P('ep'), may hold values from -0.125 to 0.125
- expert_down: bfloat16 [32, 1024, 2048], P('ep'), may hold values from -0.1875 to 0.1875
- route_group: int32 [32], P('ep'), may hold values from 0 to 3
- route_member: int32 [32, 2], P('ep'), may hold values from 0 to 7, as said below
- group_weight: float32 [32], P('ep'), may hold values from 0.25 to 1
- member_weight: float32 [32, 2], P('ep'), may hold values from 0.1 to 1
Outputs:
- layer_out: bfloat16 [32, 2048], P('ep')
- next_matrix: float32 [32, 4, 512, 512], P('ep')
- next_norm: float32 [32, 4, 512], P('ep')
- next_max: float32 [32, 4], P('ep')
Inputs may be any that keep to these rules, and one draw needn't show every extreme that they name: A row's 2 experts, numbered route_group * 8 + route_member, are different members of the one group that route_group names. No expert is named by more than 4 rows in all, and one expert is named by exactly 4 rows.
All inputs are finite; a program needn't handle non-finite values.
Results may differ from a plain program's by a relative error of at most 0.013.
Values may be sent and summed in bfloat16 or wider, within the bound.
No kernel may reach another device: no remote copies, remote signals or barrier semaphores. Data moves between devices by JAX's collectives and lax.ppermute only.
A program may use at most 64 MiB of HBM per device.

v0:
```python
import jax
import jax.numpy as jnp
from jax import lax
from jax.sharding import PartitionSpec as P

GROUPS = 4
CAPACITY = 4
norm_eps = 1e-06


def root_norm(values, gain):
    return values * lax.rsqrt(jnp.mean(values * values, axis=-1, keepdims=True) + norm_eps) * gain


def run_expert(slot_rows, gate_mat, up_mat, down_mat):
    gate_part = jnp.dot(slot_rows, gate_mat, preferred_element_type=jnp.float32)
    up_part = jnp.dot(slot_rows, up_mat, preferred_element_type=jnp.float32)
    hidden = (jax.nn.silu(gate_part) * up_part).astype(jnp.bfloat16)
    return jnp.dot(hidden, down_mat, preferred_element_type=jnp.float32).astype(jnp.bfloat16)


def local(
    tokens,
    mixer_gain,
    query_weight,
    key_weight,
    value_weight,
    outgate_weight,
    input_weight,
    forget_weight,
    forget_bias,
    memory_matrix,
    memory_norm,
    memory_max,
    mixer_out,
    expert_gain,
    expert_gate,
    expert_up,
    expert_down,
    route_group,
    route_member,
    group_weight,
    member_weight,
):
    devices = lax.axis_size("ep")
    local_rows = tokens.shape[0]
    width = tokens.shape[1]
    columns = query_weight.shape[1]
    heads = memory_matrix.shape[1]
    head_dim = memory_matrix.shape[2]
    members = devices * expert_gate.shape[0] // GROUPS
    stacked = jnp.concatenate([query_weight, key_weight, value_weight, outgate_weight], axis=1)
    piece = lax.all_gather(tokens, "ep", axis=0, tiled=True)
    normed = root_norm(piece.astype(jnp.float32), mixer_gain).astype(jnp.bfloat16)
    result = jnp.dot(normed, stacked, preferred_element_type=jnp.float32).astype(jnp.bfloat16)
    result = result.reshape(piece.shape[0], 4, columns)
    parts = lax.all_to_all(result, "ep", split_axis=0, concat_axis=2, tiled=True)
    resid = tokens.astype(jnp.float32)
    own_normed = root_norm(resid, mixer_gain).astype(jnp.bfloat16)
    input_pre = jnp.dot(own_normed, input_weight, preferred_element_type=jnp.float32)
    forget_pre = (
        jnp.dot(own_normed, forget_weight, preferred_element_type=jnp.float32) + forget_bias
    )
    log_forget = jax.nn.log_sigmoid(forget_pre)
    next_max = jnp.maximum(log_forget + memory_max, input_pre)
    keep = jnp.exp(log_forget + memory_max - next_max)
    admit = jnp.exp(input_pre - next_max)
    query_heads = parts[:, 0].astype(jnp.float32).reshape(local_rows, heads, head_dim)
    key_heads = parts[:, 1].astype(jnp.float32).reshape(local_rows, heads, head_dim) * head_dim ** (
        -0.5
    )
    value_heads = parts[:, 2].astype(jnp.float32).reshape(local_rows, heads, head_dim)
    carried = jnp.einsum(
        "shij,shj->shi", memory_matrix, query_heads, precision=lax.Precision.HIGHEST
    )
    score = jnp.sum(key_heads * query_heads, axis=-1)
    numer = keep[..., None] * carried + (admit * score)[..., None] * value_heads
    denom = keep * jnp.sum(memory_norm * query_heads, axis=-1) + admit * score
    head_out = numer / jnp.maximum(jnp.abs(denom), jnp.exp(-next_max))[..., None]
    gated = (
        head_out.reshape(local_rows, width) * jax.nn.sigmoid(parts[:, 3].astype(jnp.float32))
    ).astype(jnp.bfloat16)
    next_matrix = (
        keep[..., None, None] * memory_matrix
        + admit[..., None, None] * value_heads[..., :, None] * key_heads[..., None, :]
    )
    next_norm = keep[..., None] * memory_norm + admit[..., None] * key_heads
    proj_cols = jnp.dot(
        lax.all_gather(gated, "ep", axis=0, tiled=True),
        mixer_out,
        preferred_element_type=jnp.float32,
    ).astype(jnp.bfloat16)
    slot_index = jnp.arange(CAPACITY, dtype=jnp.int32)
    chosen_local = route_group[:, None] * members + route_member
    row_numbers = jnp.arange(local_rows, dtype=jnp.int32)
    local_weight = group_weight[:, None] * member_weight
    projected = lax.all_to_all(proj_cols, "ep", split_axis=0, concat_axis=1, tiled=True)
    middle = (resid + projected.astype(jnp.float32)).astype(jnp.bfloat16)
    expert_in = root_norm(middle.astype(jnp.float32), expert_gain).astype(jnp.bfloat16)
    targets = jnp.arange(devices, dtype=jnp.int32)
    hit = jnp.any(chosen_local[:, :, None] == targets[None, None, :], axis=1)
    outgoing = jnp.where(hit.T[:, :, None], expert_in[None, :, :], jnp.zeros((), jnp.bfloat16))
    present = hit.T.astype(jnp.bfloat16)
    incoming, flags = (
        lax.all_to_all(outgoing, "ep", split_axis=0, concat_axis=0, tiled=True),
        lax.all_to_all(present, "ep", split_axis=0, concat_axis=0, tiled=True),
    )
    flat_rows = incoming.reshape(devices * local_rows, width)
    live = (flags.reshape(devices * local_rows) > 0.5).astype(jnp.int32)
    position = jnp.cumsum(live) - 1
    select = ((position[None, :] == slot_index[:, None]) & (live[None, :] > 0)).astype(jnp.bfloat16)
    slot_rows = jnp.dot(select, flat_rows, preferred_element_type=jnp.float32).astype(jnp.bfloat16)
    finished = run_expert(slot_rows, expert_gate[0], expert_up[0], expert_down[0])
    back_rows = jnp.dot(select.T, finished, preferred_element_type=jnp.float32).astype(jnp.bfloat16)
    returned = lax.all_to_all(
        back_rows.reshape(devices, local_rows, width), "ep", split_axis=0, concat_axis=0, tiled=True
    )
    picked = returned[chosen_local.T, row_numbers[None, :]]
    mixture = jnp.sum(local_weight.T[:, :, None] * picked.astype(jnp.float32), axis=0)
    layer_out = (middle.astype(jnp.float32) + mixture).astype(jnp.bfloat16)
    return (layer_out, next_matrix, next_norm, next_max)


def solution(mesh):
    placed = (
        P("ep", None),
        P(),
        P(None, "ep"),
        P(None, "ep"),
        P(None, "ep"),
        P(None, "ep"),
        P(),
        P(),
        P(),
        P("ep", None, None, None),
        P("ep", None, None),
        P("ep", None),
        P(None, "ep"),
        P(),
        P("ep", None, None),
        P("ep", None, None),
        P("ep", None, None),
        P("ep"),
        P("ep", None),
        P("ep"),
        P("ep", None),
    )
    return jax.shard_map(
        local,
        mesh=mesh,
        in_specs=placed,
        out_specs=(P("ep", None), P("ep", None, None, None), P("ep", None, None), P("ep", None)),
        check_vma=False,
    )
```

profile of v0, /device:TPU:0, one launch (start us, length us, event | category | flops | bytes accessed | tf_op | source)
XLA Modules:
  0.0 155.1 jit_solution(15445792464496646408)
XLA Ops:
  0.6 0.0 copy-start
  0.7 0.0 copy-start.2
  0.7 0.0 copy-start.8
  0.7 0.0 copy-start.9
  0.7 0.0 copy-start.10
  0.7 0.0 copy-start.6
  0.7 0.0 copy-start.7
  0.7 0.0 copy-start.11
  0.7 44.3 %all-gather = bf16[32,1,2048]{2,1,0:T(2,128)(2,1)S(1)} all-gather(bf16[1,1,2048]{2,1,0:T(2,128)(2,1)} %bitcast.134), channel_id=1, replica_groups=mesh['ep'=32] {'ep'}, dimensions={0}, use_global_device_ids=true | all-gather | bytes 135168 | tf_op jit(solution)/shard_map/all_gather | solution.py:53
  45.1 0.3 convert_element_type.241
  45.3 0.2 fusion.30
  45.5 0.0 copy-start.4
  45.6 1.6 %convolution_convert_fusion.2 = bf16[32,256]{1,0:T(8,128)(2,1)S(1)} fusion(bf16[2048,64]{0,1:T(8,128)(2,1)} %param.26, bf16[2048,64]{0,1:T(8,128)(2,1)} %param.25, bf16[2048,64]{0,1:T(8,128)(2,1)} %param.24, bf16[2048,64]{0,1:T(8,128)(2,1)} %param.23, f32[32,1,2048]{2,1,0:T(1,128)S(1)} %convert_element_type.241, f32[2048]{0:T(1024)} %param.22, ...), kind=kOutput, calls=%fused_computation.14 | convolution fusion | flops 37953536 | bytes 1335424 | tf_op jit(solution)/shard_map/dot_general | solution.py:55
  47.2 0.1 reshape.546
  47.3 0.7 reshape.614
  48.0 2.5 %all-to-all-start = ((bf16[32,2,128]{2,1,0:T(2,128)(2,1)}), bf16[32,2,128]{2,1,0:T(2,128)(2,1)S(1)}, u32[]{:S(2)}, u32[]{:S(2)}) async-start(bf16[32,2,128]{2,1,0:T(2,128)(2,1)} %reshape.614), calls=%async_computation | async-start | bytes 32768 | tf_op jit(solution)/shard_map/all_to_all | solution.py:57
  50.6 0.6 multiply_reduce_fusion.4
  53.2 0.1 compare_reduce_fusion.1
  53.3 0.1 copy.56
  53.4 0.1 bitcast_add_fusion
  53.6 0.1 broadcast_multiply_fusion.1
  53.8 3.9 %all-to-all-done = bf16[32,2,128]{2,1,0:T(2,128)(2,1)S(1)} async-done(((bf16[32,2,128]{2,1,0:T(2,128)(2,1)}), bf16[32,2,128]{2,1,0:T(2,128)(2,1)S(1)}, u32[]{:S(2)}, u32[]{:S(2)}) %all-to-all-start) | async-done | bytes 16416 | tf_op jit(solution)/shard_map/all_to_all | solution.py:57
  57.7 0.1 reshape.615
  57.8 0.1 all_to_all.36
  57.9 0.1 multiply_reduce_fusion
  58.0 4.1 %fusion.6 = f32[4,1,512]{2,1,0:T(1,128)S(1)} fusion(bf16[4,512,1]{1,2,0:T(2,128)(2,1)S(1)} %bitcast.137, f32[1,4,512,512]{3,2,1,0:T(8,128)} %param.30), kind=kOutput, calls=%fused_computation.7 | convolution fusion | flops 12582912 | bytes 4206592 | tf_op jit(solution)/shard_map/shij,shj->shi/dot_general | solution.py:73
  62.2 0.8 multiply_reduce_fusion.3
  63.0 0.1 broadcast_multiply_fusion
  63.1 38.6 %all-gather.1 = bf16[32,1,2048]{2,1,0:T(2,128)(2,1)S(1)} all-gather(bf16[1,1,2048]{2,1,0:T(2,128)(2,1)S(1)} %convert_bitcast_fusion), channel_id=1, replica_groups=mesh['ep'=32] {'ep'}, dimensions={0}, use_global_device_ids=true | all-gather | bytes 135168 | tf_op jit(solution)/shard_map/all_gather | solution.py:89
  101.8 0.2 fusion.18
  102.0 0.6 copy.45
  102.6 2.5 %all-to-all-start.1 = ((bf16[32,1,64]{2,1,0:T(2,128)(2,1)}), bf16[32,1,64]{2,1,0:T(2,128)(2,1)S(1)}, u32[]{:S(2)}, u32[]{:S(2)}) async-start(bf16[32,1,64]{2,1,0:T(2,128)(2,1)} %copy.45), calls=%async_computation.1 | async-start | bytes 32768 | tf_op jit(solution)/shard_map/all_to_all | solution.py:97
  105.2 0.2 or_reduce_fusion
  105.4 0.7 copy.46
  106.1 6.2 %all-to-all-done.1 = bf16[32,1,64]{2,1,0:T(2,128)(2,1)S(1)} async-done(((bf16[32,1,64]{2,1,0:T(2,128)(2,1)}), bf16[32,1,64]{2,1,0:T(2,128)(2,1)S(1)}, u32[]{:S(2)}, u32[]{:S(2)}) %all-to-all-start.1) | async-done | bytes 4128 | tf_op jit(solution)/shard_map/all_to_all | solution.py:97
  112.3 2.6 %all-to-all-start.2 = ((bf16[32,1,1]{2,1,0:T(2,128)(2,1)}), bf16[32,1,1]{2,1,0:T(2,128)(2,1)S(1)}, u32[]{:S(2)}, u32[]{:S(2)}) async-start(bf16[32,1,1]{2,1,0:T(2,128)(2,1)} %copy.46), calls=%async_computation.2 | async-start | bytes 32768 | tf_op jit(solution)/shard_map/all_to_all | solution.py:106
  114.9 0.1 convert_reduce_fusion
  114.9 0.1 reshape.557
  115.0 0.6 multiply_reduce_fusion.1
  116.4 0.3 broadcast_select_fusion
  116.6 0.5 broadcast.318
  117.1 1.4 reduce.34
  118.5 0.7 reshape.616
  119.2 2.8 %all-to-all-done.2 = bf16[32,1,1]{2,1,0:T(2,128)(2,1)S(1)} async-done(((bf16[32,1,1]{2,1,0:T(2,128)(2,1)}), bf16[32,1,1]{2,1,0:T(2,128)(2,1)S(1)}, u32[]{:S(2)}, u32[]{:S(2)}) %all-to-all-start.2) | async-done | bytes 96 | tf_op jit(solution)/shard_map/all_to_all | solution.py:106
  122.0 3.1 %all-to-all-start.3 = ((bf16[32,2,1024]{2,1,0:T(2,128)(2,1)}), bf16[32,2,1024]{2,1,0:T(2,128)(2,1)S(1)}, u32[]{:S(2)}, u32[]{:S(2)}) async-start(bf16[32,2,1024]{2,1,0:T(2,128)(2,1)} %reshape.616), calls=%async_computation.3 | async-start | bytes 262144 | tf_op jit(solution)/shard_map/all_to_all | solution.py:105
  125.1 0.7 compare_reduce_fusion
  125.8 0.1 reduce-window.8
  125.8 0.1 add_reduce_fusion
  125.9 7.4 %all-to-all-done.3 = bf16[32,2,1024]{2,1,0:T(2,128)(2,1)S(1)} async-done(((bf16[32,2,1024]{2,1,0:T(2,128)(2,1)}), bf16[32,2,1024]{2,1,0:T(2,128)(2,1)S(1)}, u32[]{:S(2)}, u32[]{:S(2)}) %all-to-all-start.3) | async-done | bytes 131104 | tf_op jit(solution)/shard_map/all_to_all | solution.py:105
  133.3 0.1 reshape.617
  133.4 0.2 convolution_convert_fusion.1
  133.6 2.8 %fusion.4 = f32[4,1024]{1,0:T(4,128)S(1)} fusion(bf16[4,2048]{1,0:T(4,128)(2,1)S(1)} %convolution_convert_fusion.1, bf16[1,2048,1024]{2,1,0:T(8,128)(2,1)} %param.35), kind=kOutput, calls=%fused_computation.5 | convolution fusion | flops 16777216 | bytes 4227072 | tf_op jit(solution)/shard_map/dot_general | solution.py:16
  136.4 4.7 %fusion.9 = bf16[4,2048]{1,0:T(4,128)(2,1)S(1)} fusion(bf16[1,1024,2048]{2,1,0:T(8,128)(2,1)} %param.37, bf16[4,2048]{1,0:T(4,128)(2,1)S(1)} %convolution_convert_fusion.1, bf16[1,2048,1024]{2,1,0:T(8,128)(2,1)} %param.36, f32[4,1024]{1,0:T(4,128)S(1)} %fusion.4), kind=kOutput, calls=%fused_computation.12 | convolution fusion | flops 33587200 | bytes 8437760 | tf_op jit(solution)/shard_map/dot_general | solution.py:19
  141.1 0.2 fusion.8
  141.4 0.7 reduce.35
  142.0 0.7 reshape.618
  142.8 2.6 %all-to-all-start.4 = ((bf16[32,2,1024]{2,1,0:T(2,128)(2,1)}), bf16[32,2,1024]{2,1,0:T(2,128)(2,1)S(1)}, u32[]{:S(2)}, u32[]{:S(2)}) async-start(bf16[32,2,1024]{2,1,0:T(2,128)(2,1)} %reshape.618), calls=%async_computation.4 | async-start | bytes 262144 | tf_op jit(solution)/shard_map/all_to_all | solution.py:115
  145.3 4.7 %multiply_add_fusion = f32[1,4,512,512]{3,2,1,0:T(8,128)} fusion(f32[1,4,512,512]{3,2,1,0:T(8,128)} %param.30, f32[4,512]{1,0:T(4,128)S(1)} %mul.289, f32[4,512]{1,0:T(4,128)S(1)} %get-tuple-element.15, f32[4]{0:T(128)S(1)} %fusion.68), kind=kLoop, calls=%fused_computation.9 | loop fusion | flops 3145728 | bytes 8405008 | tf_op jit(solution)/shard_map/add | solution.py:84
  150.1 3.5 %all-to-all-done.4 = bf16[32,2,1024]{2,1,0:T(2,128)(2,1)S(1)} async-done(((bf16[32,2,1024]{2,1,0:T(2,128)(2,1)}), bf16[32,2,1024]{2,1,0:T(2,128)(2,1)S(1)}, u32[]{:S(2)}, u32[]{:S(2)}) %all-to-all-start.4) | async-done | bytes 131104 | tf_op jit(solution)/shard_map/all_to_all | solution.py:115
  153.5 0.1 reshape.619
  153.6 0.1 copy.50
  153.7 0.6 gather_fusion
  154.4 0.1 fusion.40
  154.5 0.6 add_convert_fusion
  (33 shorter events, 0.3 us)
Async XLA Ops:
  0.6 101.1 %copy-start = (bf16[2048,64]{0,1:T(8,128)(2,1)S(1)}, bf16[2048,64]{0,1:T(8,128)(2,1)}, u32[]{:S(2)}) copy-start(bf16[2048,64]{0,1:T(8,128)(2,1)} %param.33) | copy-start | bytes 786436
  0.6 49.9 %copy-start.1 = (bf16[1,2048]{1,0:T(2,128)(2,1)S(1)}, bf16[1,2048]{1,0:T(2,128)(2,1)}, u32[]{:S(2)}) copy-start(bf16[1,2048]{1,0:T(2,128)(2,1)} %param.21) | copy-start | bytes 12292
  0.7 52.7 %copy-start.2 = (f32[2048]{0:T(1024)S(1)}, f32[2048]{0:T(1024)}, u32[]{:S(2)}) copy-start(f32[2048]{0:T(1024)} %param.22) | copy-start | bytes 24580
  0.7 51.2 %copy-start.8 = (s32[1,2]{1,0:T(1,128)S(1)}, s32[1,2]{1,0:T(1,128)}, u32[]{:S(2)}) copy-start(s32[1,2]{1,0:T(1,128)} %param.39) | copy-start | bytes 28
  0.7 52.7 %copy-start.9 = (f32[1,4]{1,0:T(1,128)S(1)}, f32[1,4]{1,0:T(1,128)}, u32[]{:S(2)}) copy-start(f32[1,4]{1,0:T(1,128)} %param.32) | copy-start | bytes 52
  0.7 52.7 %copy-start.10 = (f32[4]{0:T(128)S(1)}, f32[4]{0:T(128)}, u32[]{:S(2)}) copy-start(f32[4]{0:T(128)} %param.29) | copy-start | bytes 52
  0.7 52.7 %copy-start.6 = (bf16[2048,4]{0,1:T(4,128)(2,1)S(1)}, bf16[2048,4]{0,1:T(4,128)(2,1)}, u32[]{:S(2)}) copy-start(bf16[2048,4]{0,1:T(4,128)(2,1)} %param.28) | copy-start | bytes 49156
  0.7 52.9 %copy-start.7 = (bf16[2048,4]{0,1:T(4,128)(2,1)S(1)}, bf16[2048,4]{0,1:T(4,128)(2,1)}, u32[]{:S(2)}) copy-start(bf16[2048,4]{0,1:T(4,128)(2,1)} %param.27) | copy-start | bytes 49156
  0.7 53.0 %copy-start.11 = (f32[1,2]{1,0:T(1,128)S(1)}, f32[1,2]{1,0:T(1,128)}, u32[]{:S(2)}) copy-start(f32[1,2]{1,0:T(1,128)} %param.41) | copy-start | bytes 28
  45.5 16.6 %copy-start.3 = (f32[1,4,512]{2,1,0:T(4,128)S(1)}, f32[1,4,512]{2,1,0:T(4,128)}, u32[]{:S(2)}) copy-start(f32[1,4,512]{2,1,0:T(4,128)} %param.31) | copy-start | bytes 24580
  45.5 70.8 %copy-start.4 = (f32[2048]{0:T(1024)S(1)}, f32[2048]{0:T(1024)}, u32[]{:S(2)}) copy-start(f32[2048]{0:T(1024)} %param.34) | copy-start | bytes 24580
  48.0 9.7 %all-to-all-start = ((bf16[32,2,128]{2,1,0:T(2,128)(2,1)}), bf16[32,2,128]{2,1,0:T(2,128)(2,1)S(1)}, u32[]{:S(2)}, u32[]{:S(2)}) async-start(bf16[32,2,128]{2,1,0:T(2,128)(2,1)} %reshape.614), calls=%async_computation | async-start | bytes 32768 | tf_op jit(solution)/shard_map/all_to_all | solution.py:57
  53.7 82.7 %copy-start.5 = (f32[1,4]{1,0:T(1,128)}, f32[1,4]{1,0:T(1,128)S(1)}, u32[]{:S(2)}) copy-start(f32[1,4]{1,0:T(1,128)S(1)} %get-tuple-element.11) | copy-start | bytes 52
  102.6 9.7 %all-to-all-start.1 = ((bf16[32,1,64]{2,1,0:T(2,128)(2,1)}), bf16[32,1,64]{2,1,0:T(2,128)(2,1)S(1)}, u32[]{:S(2)}, u32[]{:S(2)}) async-start(bf16[32,1,64]{2,1,0:T(2,128)(2,1)} %copy.45), calls=%async_computation.1 | async-start | bytes 32768 | tf_op jit(solution)/shard_map/all_to_all | solution.py:97
  112.3 9.7 %all-to-all-start.2 = ((bf16[32,1,1]{2,1,0:T(2,128)(2,1)}), bf16[32,1,1]{2,1,0:T(2,128)(2,1)S(1)}, u32[]{:S(2)}, u32[]{:S(2)}) async-start(bf16[32,1,1]{2,1,0:T(2,128)(2,1)} %copy.46), calls=%async_computation.2 | async-start | bytes 32768 | tf_op jit(solution)/shard_map/all_to_all | solution.py:106
  122.0 11.3 %all-to-all-start.3 = ((bf16[32,2,1024]{2,1,0:T(2,128)(2,1)}), bf16[32,2,1024]{2,1,0:T(2,128)(2,1)S(1)}, u32[]{:S(2)}, u32[]{:S(2)}) async-start(bf16[32,2,1024]{2,1,0:T(2,128)(2,1)} %reshape.616), calls=%async_computation.3 | async-start | bytes 262144 | tf_op jit(solution)/shard_map/all_to_all | solution.py:105
  142.8 10.8 %all-to-all-start.4 = ((bf16[32,2,1024]{2,1,0:T(2,128)(2,1)}), bf16[32,2,1024]{2,1,0:T(2,128)(2,1)S(1)}, u32[]{:S(2)}, u32[]{:S(2)}) async-start(bf16[32,2,1024]{2,1,0:T(2,128)(2,1)} %reshape.618), calls=%async_computation.4 | async-start | bytes 262144 | tf_op jit(solution)/shard_map/all_to_all | solution.py:115
where the time goes:
time: 156 us; the launch traced here: 155 us
  blocking collectives  83 us (53%)
  waiting for transfers between devices  23.7 us (15%)
  matrix products  14.3 us (9%)
  starting transfers between devices  13.3 us (9%)
  other arithmetic  11.7 us (8%)
  local copies, waits for them, and re-layouts  5.47 us (4%)
  between operations  3.69 us (2%)
    all_gather x1, blocking collectives, local(): piece = lax.all_gather(tokens, 'ep', axis=0, tiled=True)  44.3 us
    all_gather x1, blocking collectives, local(): lax.all_gather(gated, 'ep', axis=0, tiled=True)  38.6 us
    all_to_all x1, waiting for transfers between devices, local(): lax.all_to_all(outgoing, 'ep', split_axis=0, concat_axis=0, tiled=True)  7.35 us
    all_to_all x1, waiting for transfers between devices, local(): lax.all_to_all(proj_cols, 'ep', split_axis=0, concat_axis=1, tiled=True)  6.21 us
    add x1, other arithmetic, local(): keep[..., None, None] * memory_matrix  4.74 us
    dot_general x1, matrix products, run_expert(): jnp.dot(hidden, down_mat, preferred_element_type=jnp.float32)  4.68 us
    dot_general x1, matrix products, local(): jnp.einsum('shij,shj->shi', memory_matrix, query_heads, precision=lax.Pre...  4.15 us
    all_to_all x1, waiting for transfers between devices, local(): lax.all_to_all(result, 'ep', split_axis=0, concat_axis=2, tiled=True)  3.87 us
  transfers between devices with their start and end apart: 5, of which 5 were waited for; matrix products, arithmetic and copies ran while one was open for 7% of the time, Pallas kernels for 0%

commit v1 on v0

--- a/solution.py
+++ b/solution.py
@@ -94,7 +94,10 @@
     chosen_local = route_group[:, None] * members + route_member
     row_numbers = jnp.arange(local_rows, dtype=jnp.int32)
     local_weight = group_weight[:, None] * member_weight
-    projected = lax.all_to_all(proj_cols, "ep", split_axis=0, concat_axis=1, tiled=True)
+    projected = jnp.concatenate(
+        lax.all_to_all(jnp.stack(jnp.split(proj_cols, lax.axis_size("ep"), axis=0)), "ep", 0, 0),
+        axis=1,
+    )
     middle = (resid + projected.astype(jnp.float32)).astype(jnp.bfloat16)
     expert_in = root_norm(middle.astype(jnp.float32), expert_gain).astype(jnp.bfloat16)
     targets = jnp.arange(devices, dtype=jnp.int32)

time: 156 us -> 171 us (1.096)
  local copies, waits for them, and re-layouts: 5.47 us -> 21.3 us
    unnamed x32 -> x63, local copies, waits for them, and re-layouts: 2.59 us -> 18.5 us
where the time goes in v1:
time: 171 us
  blocking collectives  83 us (49%)
  waiting for transfers between devices  23.7 us (14%)
  local copies, waits for them, and re-layouts  21.3 us (12%)
  matrix products  14.2 us (8%)
  starting transfers between devices  13.3 us (8%)
  other arithmetic  11.7 us (7%)
  between operations  3.71 us (2%)
    all_gather x1, blocking collectives, local(): piece = lax.all_gather(tokens, 'ep', axis=0, tiled=True)  44.3 us
    all_gather x1, blocking collectives, local(): lax.all_gather(gated, 'ep', axis=0, tiled=True)  38.6 us
    unnamed x63, local copies, waits for them, and re-layouts  18.5 us
    all_to_all x1, waiting for transfers between devices, local(): lax.all_to_all(outgoing, 'ep', split_axis=0, concat_axis=0, tiled=True)  7.35 us
    all_to_all x1, waiting for transfers between devices, local(): lax.all_to_all(jnp.stack(jnp.split(proj_cols, lax.axis_size('ep'), axis=0...  6.21 us
    add x1, other arithmetic, local(): keep[..., None, None] * memory_matrix  4.74 us
    dot_general x1, matrix products, run_expert(): jnp.dot(hidden, down_mat, preferred_element_type=jnp.float32)  4.68 us
    dot_general x1, matrix products, local(): jnp.einsum('shij,shj->shi', memory_matrix, query_heads, precision=lax.Pre...  4.15 us
  transfers between devices with their start and end apart: 5, of which 5 were waited for; matrix products, arithmetic and copies ran while one was open for 7% of the time, Pallas kernels for 0%

profile of v1, /device:TPU:0, one launch (start us, length us, event | category | flops | bytes accessed | tf_op | source)
XLA Modules:
  0.0 170.9 jit_solution(8038498227252386467)
XLA Ops:
  0.7 44.3 %all-gather = bf16[32,1,2048]{2,1,0:T(2,128)(2,1)S(1)} all-gather(bf16[1,1,2048]{2,1,0:T(2,128)(2,1)} %bitcast.260), channel_id=1, replica_groups=mesh['ep'=32] {'ep'}, dimensions={0}, use_global_device_ids=true | all-gather | bytes 135168 | tf_op jit(solution)/shard_map/all_gather | solution.py:53
  45.1 0.3 convert_element_type.241
  45.6 1.6 convolution_convert_fusion.2
  47.3 0.7 reshape.609
  48.0 2.5 %all-to-all-start = ((bf16[32,2,128]{2,1,0:T(2,128)(2,1)}), bf16[32,2,128]{2,1,0:T(2,128)(2,1)S(1)}, u32[]{:S(2)}, u32[]{:S(2)}) async-start(bf16[32,2,128]{2,1,0:T(2,128)(2,1)} %reshape.609), calls=%async_computation | async-start | bytes 32768 | tf_op jit(solution)/shard_map/all_to_all | solution.py:57
  50.6 0.6 multiply_reduce_fusion.4
  53.8 3.9 %all-to-all-done = bf16[32,2,128]{2,1,0:T(2,128)(2,1)S(1)} async-done(((bf16[32,2,128]{2,1,0:T(2,128)(2,1)}), bf16[32,2,128]{2,1,0:T(2,128)(2,1)S(1)}, u32[]{:S(2)}, u32[]{:S(2)}) %all-to-all-start) | async-done | bytes 16416 | tf_op jit(solution)/shard_map/all_to_all | solution.py:57
  58.0 4.1 %fusion.6 = f32[4,1,512]{2,1,0:T(1,128)S(1)} fusion(bf16[4,512,1]{1,2,0:T(2,128)(2,1)S(1)} %bitcast.263, f32[1,4,512,512]{3,2,1,0:T(8,128)} %param.30), kind=kOutput, calls=%fused_computation.7 | convolution fusion | flops 12582912 | bytes 4206592 | tf_op jit(solution)/shard_map/shij,shj->shi/dot_general | solution.py:73
  62.2 0.8 multiply_reduce_fusion.3
  63.1 38.6 %all-gather.1 = bf16[32,1,2048]{2,1,0:T(2,128)(2,1)S(1)} all-gather(bf16[1,1,2048]{2,1,0:T(2,128)(2,1)S(1)} %convert_bitcast_fusion), channel_id=1, replica_groups=mesh['ep'=32] {'ep'}, dimensions={0}, use_global_device_ids=true | all-gather | bytes 135168 | tf_op jit(solution)/shard_map/all_gather | solution.py:89
  102.0 0.5 constant_dynamic-update-slice_fusion.31
  102.5 0.5 constant_dynamic-update-slice_fusion.30
  103.0 0.5 constant_dynamic-update-slice_fusion.29
  103.5 0.5 constant_dynamic-update-slice_fusion.28
  104.1 0.5 constant_dynamic-update-slice_fusion.27
  104.6 0.5 constant_dynamic-update-slice_fusion.26
  105.1 0.5 constant_dynamic-update-slice_fusion.25
  105.6 0.5 constant_dynamic-update-slice_fusion.24
  106.1 0.5 constant_dynamic-update-slice_fusion.23
  106.6 0.5 constant_dynamic-update-slice_fusion.22
  107.2 0.5 constant_dynamic-update-slice_fusion.21
  107.7 0.5 constant_dynamic-update-slice_fusion.20
  108.2 0.5 constant_dynamic-update-slice_fusion.19
  108.7 0.5 constant_dynamic-update-slice_fusion.18
  109.2 0.5 constant_dynamic-update-slice_fusion.17
  109.7 0.5 constant_dynamic-update-slice_fusion.16
  110.2 0.5 constant_dynamic-update-slice_fusion.15
  110.8 0.5 constant_dynamic-update-slice_fusion.14
  111.3 0.5 constant_dynamic-update-slice_fusion.13
  111.8 0.5 constant_dynamic-update-slice_fusion.12
  112.3 0.5 constant_dynamic-update-slice_fusion.11
  112.8 0.5 constant_dynamic-update-slice_fusion.10
  113.3 0.5 constant_dynamic-update-slice_fusion.9
  113.8 0.5 constant_dynamic-update-slice_fusion.8
  114.4 0.5 constant_dynamic-update-slice_fusion.7
  114.9 0.5 constant_dynamic-update-slice_fusion.6
  115.4 0.5 constant_dynamic-update-slice_fusion.5
  115.9 0.5 constant_dynamic-update-slice_fusion.4
  116.4 0.5 constant_dynamic-update-slice_fusion.3
  116.9 0.5 constant_dynamic-update-slice_fusion.2
  117.4 0.5 constant_dynamic-update-slice_fusion.1
  118.0 0.5 constant_dynamic-update-slice_fusion
  118.5 2.5 %all-to-all-start.1 = ((bf16[32,1,64]{2,1,0:T(2,128)(2,1)}), bf16[32,1,64]{2,1,0:T(2,128)(2,1)S(1)}, u32[]{:S(2)}, u32[]{:S(2)}) async-start(bf16[32,1,64]{2,1,0:T(2,128)(2,1)} %constant_dynamic-update-slice_fusion), calls=%async_computation.1 | async-start | bytes 32768 | tf_op jit(solution)/shard_map/all_to_all | solution.py:98
  121.2 0.7 copy.43
  121.9 6.2 %all-to-all-done.1 = bf16[32,1,64]{2,1,0:T(2,128)(2,1)S(1)} async-done(((bf16[32,1,64]{2,1,0:T(2,128)(2,1)}), bf16[32,1,64]{2,1,0:T(2,128)(2,1)S(1)}, u32[]{:S(2)}, u32[]{:S(2)}) %all-to-all-start.1) | async-done | bytes 4128 | tf_op jit(solution)/shard_map/all_to_all | solution.py:98
  128.1 2.6 %all-to-all-start.2 = ((bf16[32,1,1]{2,1,0:T(2,128)(2,1)}), bf16[32,1,1]{2,1,0:T(2,128)(2,1)S(1)}, u32[]{:S(2)}, u32[]{:S(2)}) async-start(bf16[32,1,1]{2,1,0:T(2,128)(2,1)} %copy.43), calls=%async_computation.2 | async-start | bytes 32768 | tf_op jit(solution)/shard_map/all_to_all | solution.py:109
  130.8 0.6 multiply_reduce_fusion.1
  132.2 0.3 broadcast_select_fusion
  132.5 0.5 broadcast.318
  133.0 1.4 reduce.34
  134.4 0.7 reshape.611
  135.1 2.8 %all-to-all-done.2 = bf16[32,1,1]{2,1,0:T(2,128)(2,1)S(1)} async-done(((bf16[32,1,1]{2,1,0:T(2,128)(2,1)}), bf16[32,1,1]{2,1,0:T(2,128)(2,1)S(1)}, u32[]{:S(2)}, u32[]{:S(2)}) %all-to-all-start.2) | async-done | bytes 96 | tf_op jit(solution)/shard_map/all_to_all | solution.py:109
  137.9 3.1 %all-to-all-start.3 = ((bf16[32,2,1024]{2,1,0:T(2,128)(2,1)}), bf16[32,2,1024]{2,1,0:T(2,128)(2,1)S(1)}, u32[]{:S(2)}, u32[]{:S(2)}) async-start(bf16[32,2,1024]{2,1,0:T(2,128)(2,1)} %reshape.611), calls=%async_computation.3 | async-start | bytes 262144 | tf_op jit(solution)/shard_map/all_to_all | solution.py:108
  140.9 0.7 compare_reduce_fusion
  141.8 7.4 %all-to-all-done.3 = bf16[32,2,1024]{2,1,0:T(2,128)(2,1)S(1)} async-done(((bf16[32,2,1024]{2,1,0:T(2,128)(2,1)}), bf16[32,2,1024]{2,1,0:T(2,128)(2,1)S(1)}, u32[]{:S(2)}, u32[]{:S(2)}) %all-to-all-start.3) | async-done | bytes 131104 | tf_op jit(solution)/shard_map/all_to_all | solution.py:108
  149.4 2.8 %fusion.4 = f32[4,1024]{1,0:T(4,128)S(1)} fusion(bf16[4,2048]{1,0:T(4,128)(2,1)S(1)} %convolution_convert_fusion.1, bf16[1,2048,1024]{2,1,0:T(8,128)(2,1)} %param.35), kind=kOutput, calls=%fused_computation.5 | convolution fusion | flops 16777216 | bytes 4227072 | tf_op jit(solution)/shard_map/dot_general | solution.py:16
  152.3 4.7 %fusion.9 = bf16[4,2048]{1,0:T(4,128)(2,1)S(1)} fusion(bf16[1,1024,2048]{2,1,0:T(8,128)(2,1)} %param.37, bf16[4,2048]{1,0:T(4,128)(2,1)S(1)} %convolution_convert_fusion.1, bf16[1,2048,1024]{2,1,0:T(8,128)(2,1)} %param.36, f32[4,1024]{1,0:T(4,128)S(1)} %fusion.4), kind=kOutput, calls=%fused_computation.12 | convolution fusion | flops 33587200 | bytes 8437760 | tf_op jit(solution)/shard_map/dot_general | solution.py:19
  157.2 0.7 reduce.35
  157.9 0.7 reshape.613
  158.6 2.6 %all-to-all-start.4 = ((bf16[32,2,1024]{2,1,0:T(2,128)(2,1)}), bf16[32,2,1024]{2,1,0:T(2,128)(2,1)S(1)}, u32[]{:S(2)}, u32[]{:S(2)}) async-start(bf16[32,2,1024]{2,1,0:T(2,128)(2,1)} %reshape.613), calls=%async_computation.4 | async-start | bytes 262144 | tf_op jit(solution)/shard_map/all_to_all | solution.py:118
  161.2 4.7 %multiply_add_fusion = f32[1,4,512,512]{3,2,1,0:T(8,128)} fusion(f32[1,4,512,512]{3,2,1,0:T(8,128)} %param.30, f32[4,512]{1,0:T(4,128)S(1)} %mul.289, f32[4,512]{1,0:T(4,128)S(1)} %get-tuple-element.15, f32[4]{0:T(128)S(1)} %fusion.67), kind=kLoop, calls=%fused_computation.9 | loop fusion | flops 3145728 | bytes 8405008 | tf_op jit(solution)/shard_map/add | solution.py:84
  165.9 3.5 %all-to-all-done.4 = bf16[32,2,1024]{2,1,0:T(2,128)(2,1)S(1)} async-done(((bf16[32,2,1024]{2,1,0:T(2,128)(2,1)}), bf16[32,2,1024]{2,1,0:T(2,128)(2,1)S(1)}, u32[]{:S(2)}, u32[]{:S(2)}) %all-to-all-start.4) | async-done | bytes 131104 | tf_op jit(solution)/shard_map/all_to_all | solution.py:118
  169.6 0.6 gather_fusion
  170.3 0.6 add_convert_fusion
  (64 shorter events, 2.9 us)
Async XLA Ops:
  0.6 101.1 %copy-start = (bf16[2048,64]{0,1:T(8,128)(2,1)S(1)}, bf16[2048,64]{0,1:T(8,128)(2,1)}, u32[]{:S(2)}) copy-start(bf16[2048,64]{0,1:T(8,128)(2,1)} %param.33) | copy-start | bytes 786436
  0.6 49.9 %copy-start.1 = (bf16[1,2048]{1,0:T(2,128)(2,1)S(1)}, bf16[1,2048]{1,0:T(2,128)(2,1)}, u32[]{:S(2)}) copy-start(bf16[1,2048]{1,0:T(2,128)(2,1)} %param.21) | copy-start | bytes 12292
  0.7 52.7 %copy-start.2 = (f32[2048]{0:T(1024)S(1)}, f32[2048]{0:T(1024)}, u32[]{:S(2)}) copy-start(f32[2048]{0:T(1024)} %param.22) | copy-start | bytes 24580
  0.7 51.2 %copy-start.8 = (s32[1,2]{1,0:T(1,128)S(1)}, s32[1,2]{1,0:T(1,128)}, u32[]{:S(2)}) copy-start(s32[1,2]{1,0:T(1,128)} %param.39) | copy-start | bytes 28
  0.7 52.7 %copy-start.9 = (f32[1,4]{1,0:T(1,128)S(1)}, f32[1,4]{1,0:T(1,128)}, u32[]{:S(2)}) copy-start(f32[1,4]{1,0:T(1,128)} %param.32) | copy-start | bytes 52
  0.7 52.7 %copy-start.10 = (f32[4]{0:T(128)S(1)}, f32[4]{0:T(128)}, u32[]{:S(2)}) copy-start(f32[4]{0:T(128)} %param.29) | copy-start | bytes 52
  0.7 52.7 %copy-start.6 = (bf16[2048,4]{0,1:T(4,128)(2,1)S(1)}, bf16[2048,4]{0,1:T(4,128)(2,1)}, u32[]{:S(2)}) copy-start(bf16[2048,4]{0,1:T(4,128)(2,1)} %param.28) | copy-start | bytes 49156
  0.7 52.9 %copy-start.7 = (bf16[2048,4]{0,1:T(4,128)(2,1)S(1)}, bf16[2048,4]{0,1:T(4,128)(2,1)}, u32[]{:S(2)}) copy-start(bf16[2048,4]{0,1:T(4,128)(2,1)} %param.27) | copy-start | bytes 49156
  0.7 53.0 %copy-start.11 = (f32[1,2]{1,0:T(1,128)S(1)}, f32[1,2]{1,0:T(1,128)}, u32[]{:S(2)}) copy-start(f32[1,2]{1,0:T(1,128)} %param.41) | copy-start | bytes 28
  45.5 16.6 %copy-start.3 = (f32[1,4,512]{2,1,0:T(4,128)S(1)}, f32[1,4,512]{2,1,0:T(4,128)}, u32[]{:S(2)}) copy-start(f32[1,4,512]{2,1,0:T(4,128)} %param.31) | copy-start | bytes 24580
  45.5 86.6 %copy-start.4 = (f32[2048]{0:T(1024)S(1)}, f32[2048]{0:T(1024)}, u32[]{:S(2)}) copy-start(f32[2048]{0:T(1024)} %param.34) | copy-start | bytes 24580
  48.0 9.7 %all-to-all-start = ((bf16[32,2,128]{2,1,0:T(2,128)(2,1)}), bf16[32,2,128]{2,1,0:T(2,128)(2,1)S(1)}, u32[]{:S(2)}, u32[]{:S(2)}) async-start(bf16[32,2,128]{2,1,0:T(2,128)(2,1)} %reshape.609), calls=%async_computation | async-start | bytes 32768 | tf_op jit(solution)/shard_map/all_to_all | solution.py:57
  53.7 98.6 %copy-start.5 = (f32[1,4]{1,0:T(1,128)}, f32[1,4]{1,0:T(1,128)S(1)}, u32[]{:S(2)}) copy-start(f32[1,4]{1,0:T(1,128)S(1)} %get-tuple-element.11) | copy-start | bytes 52
  118.5 9.7 %all-to-all-start.1 = ((bf16[32,1,64]{2,1,0:T(2,128)(2,1)}), bf16[32,1,64]{2,1,0:T(2,128)(2,1)S(1)}, u32[]{:S(2)}, u32[]{:S(2)}) async-start(bf16[32,1,64]{2,1,0:T(2,128)(2,1)} %constant_dynamic-update-slice_fusion), calls=%async_computation.1 | async-start | bytes 32768 | tf_op jit(solution)/shard_map/all_to_all | solution.py:98
  128.1 9.7 %all-to-all-start.2 = ((bf16[32,1,1]{2,1,0:T(2,128)(2,1)}), bf16[32,1,1]{2,1,0:T(2,128)(2,1)S(1)}, u32[]{:S(2)}, u32[]{:S(2)}) async-start(bf16[32,1,1]{2,1,0:T(2,128)(2,1)} %copy.43), calls=%async_computation.2 | async-start | bytes 32768 | tf_op jit(solution)/shard_map/all_to_all | solution.py:109
  137.9 11.3 %all-to-all-start.3 = ((bf16[32,2,1024]{2,1,0:T(2,128)(2,1)}), bf16[32,2,1024]{2,1,0:T(2,128)(2,1)S(1)}, u32[]{:S(2)}, u32[]{:S(2)}) async-start(bf16[32,2,1024]{2,1,0:T(2,128)(2,1)} %reshape.611), calls=%async_computation.3 | async-start | bytes 262144 | tf_op jit(solution)/shard_map/all_to_all | solution.py:108
  158.6 10.8 %all-to-all-start.4 = ((bf16[32,2,1024]{2,1,0:T(2,128)(2,1)}), bf16[32,2,1024]{2,1,0:T(2,128)(2,1)S(1)}, u32[]{:S(2)}, u32[]{:S(2)}) async-start(bf16[32,2,1024]{2,1,0:T(2,128)(2,1)} %reshape.613), calls=%async_computation.4 | async-start | bytes 262144 | tf_op jit(solution)/shard_map/all_to_all | solution.py:118
